TPU v7x, 512 devices: a whole 4x4x16 slice. The times are simulated.
512 devices in a mesh: fs: 16 (over y, x), tp: 32 (over z, core).
Axes of the slice: x: 4, y: 4, z: 16, core: 2. Of those that a mesh axis runs over, the one named last changes fastest.
Arguments:
- value_input: bfloat16 [32768, 2048], P('fs', 'tp'), may hold values from -50 to 50
- value_cotangent: bfloat16 [32768, 512], P('fs'), may hold values from -6 to 6
- value_factor: bfloat16 [512, 128], replicated, may hold values from -10 to 10
- value_master: float32 [512, 2048], P('fs', 'tp'), may hold values from -0.125 to 0.125
- value_first: float32 [128, 2048], P('fs', 'tp'), may hold values from -4 to 4
- value_second: float32 [128, 2048], P('fs', 'tp'), may hold values from 0.01 to 0.2
- mixed_heads: bfloat16 [32768, 1024], P('fs', 'tp'), may hold values from -6 to 6
- output_cotangent: bfloat16 [32768, 2048], P('fs', 'tp'), may hold values from -50 to 50
- output_factor: bfloat16 [1024, 128], replicated, may hold values from -10 to 10
- output_master: float32 [1024, 2048], P('fs', 'tp'), may hold values from -0.1875 to 0.1875
- output_first: float32 [128, 2048], P('fs', 'tp'), may hold values from -4 to 4
- output_second: float32 [128, 2048], P('fs', 'tp'), may hold values from 0.01 to 0.2
Outputs:
- value_step: float32 [512, 2048], P('fs', 'tp')
- value_new_master: float32 [512, 2048], P('fs', 'tp')
- value_copy: bfloat16 [512, 2048], P(None, 'tp')
- value_first_new: float32 [128, 2048], P('fs', 'tp')
- value_second_new: float32 [128, 2048], P('fs', 'tp')
- output_step: float32 [1024, 2048], P('fs', 'tp')
- output_new_master: float32 [1024, 2048], P('fs', 'tp')
- output_copy: bfloat16 [1024, 2048], P(None, 'tp')
- output_first_new: float32 [128, 2048], P('fs', 'tp')
- output_second_new: float32 [128, 2048], P('fs', 'tp')
All inputs are finite; a program needn't handle non-finite values.
Results may differ from a plain program's by a relative error of at most 0.001.
Values may be sent and summed in bfloat16 or wider, within the bound.
A program may use at most 64 MiB of HBM per device.

v0:
```python
import jax
import jax.numpy as jnp
from jax import lax
from jax.sharding import Mesh
from jax.sharding import PartitionSpec as P

FS = ("fs_0", "fs_1")
TP = ("tp_0", "tp_1")
FS_TP = ("fs_0", "fs_1", "tp_0", "tp_1")


highest = lax.Precision.HIGHEST


def split_up(x, dim, count):
    dims = x.shape
    tiles = x.reshape(*dims[:dim], count, dims[dim] // count, *dims[dim + 1 :])
    return jnp.moveaxis(tiles, dim, 0)


def summed_on_arrival(x, axis, dim):
    count = lax.axis_size(axis)
    tiles = lax.all_to_all(split_up(x, dim, count), axis, 0, 0, tiled=True)
    return jnp.sum(tiles, axis=0)


def by_axis(x, axes):
    for axis in axes:
        x = lax.psum(x, axis)
    return x


def in_one_piece(arrays, axis, dim, along):
    both = jnp.concatenate(arrays, axis=along)
    whole, at, outs = (lax.all_gather(both, axis, axis=dim, tiled=True), 0, [])
    for a in arrays:
        outs.append(lax.slice_in_dim(whole, at, at + a.shape[along], axis=along))
        at += a.shape[along]
    return tuple(outs)


def joined_along(tiles, dim):
    dims = list(tiles.shape[1:])
    dims[dim] *= tiles.shape[0]
    return jnp.moveaxis(tiles, 0, dim).reshape(dims)


def gather_packed(arrays, axis, dims):
    flat = jnp.concatenate([a.reshape(-1) for a in arrays])
    lines, at, outs = (lax.all_gather(flat, axis), 0, [])
    for a, dim in zip(arrays, dims):
        tiles = lines[:, at : at + a.size].reshape(-1, *a.shape)
        outs.append(joined_along(tiles, dim))
        at += a.size
    return tuple(outs)


def tokens_exact(left, right):
    return lax.dot_general(
        left, right, (((0,), (0,)), ((), ())), precision=highest, preferred_element_type=jnp.float32
    )


def moment_update(projected, scale, first, second):
    scaled = scale * projected
    first_new = 0.9 * first + 0.1 * scaled
    second_new = 0.95 * second + 0.05 * scaled * scaled
    direction = first_new / (jnp.sqrt(second_new) + 1e-08)
    return (first_new, second_new, direction)


def project_both(value_image, output_image, value_input, output_cotangent, band):
    value_wide = value_input.astype(jnp.float32)
    output_wide = output_cotangent.astype(jnp.float32)
    columns = value_input.shape[1]
    blocks = 2 * band * lax.axis_size(FS) // (2 * band)
    value_term = tokens_exact(value_image, value_wide).reshape(blocks, band, columns)
    output_term = tokens_exact(output_image, output_wide).reshape(blocks, band, columns)
    paired = summed_on_arrival(
        jnp.stack([value_term, output_term], axis=1).reshape(2 * band * lax.axis_size(FS), columns),
        FS,
        0,
    )
    return (paired[:band], paired[band:])


def on_device(
    value_input,
    value_cotangent,
    value_factor,
    value_master,
    value_first,
    value_second,
    mixed_heads,
    output_cotangent,
    output_factor,
    output_master,
    output_first,
    output_second,
):
    fs_count = lax.axis_size(FS)
    fs_place = lax.axis_index(FS)
    rank = value_factor.shape[1]
    band = rank // fs_count
    columns = value_input.shape[1]
    value_rows = value_master.shape[0]
    output_rows = output_master.shape[0]
    value_block = lax.dynamic_slice_in_dim(
        value_factor, fs_place * value_rows, value_rows, 0
    ).astype(jnp.float32)
    output_block = lax.dynamic_slice_in_dim(
        output_factor, fs_place * output_rows, output_rows, 0
    ).astype(jnp.float32)
    value_image = jnp.dot(value_cotangent, value_factor, preferred_element_type=jnp.float32)
    heads_whole = lax.all_gather(mixed_heads, TP, axis=1, tiled=True)
    output_image = jnp.dot(heads_whole, output_factor, preferred_element_type=jnp.float32)
    value_proj, output_proj = project_both(
        value_image, output_image, value_input, output_cotangent, band
    )
    total_count = rank * columns * lax.axis_size(TP)
    value_square, output_square = (
        by_axis(jnp.sum(value_proj * value_proj), FS_TP),
        by_axis(jnp.sum(output_proj * output_proj), FS_TP),
    )
    value_scale = lax.rsqrt(value_square / total_count + 1e-06)
    output_scale = lax.rsqrt(output_square / total_count + 1e-06)
    value_first_new, value_second_new, value_dir = moment_update(
        value_proj, value_scale, value_first, value_second
    )
    output_first_new, output_second_new, output_dir = moment_update(
        output_proj, output_scale, output_first, output_second
    )
    value_dir_all, output_dir_all = in_one_piece((value_dir, output_dir), FS, 0, 1)
    value_step = jnp.dot(
        value_block, value_dir_all, precision=highest, preferred_element_type=jnp.float32
    )
    output_step = jnp.dot(
        output_block, output_dir_all, precision=highest, preferred_element_type=jnp.float32
    )
    value_new = value_master - 0.002 * value_step
    output_new = output_master - 0.002 * output_step
    value_copy, output_copy = gather_packed(
        (value_new.astype(jnp.bfloat16), output_new.astype(jnp.bfloat16)), FS, (0, 0)
    )
    return (
        value_step,
        value_new,
        value_copy,
        value_first_new,
        value_second_new,
        output_step,
        output_new,
        output_copy,
        output_first_new,
        output_second_new,
    )


def solution(mesh):
    split = Mesh(mesh.devices.reshape(4, 4, 16, 2), ("fs_0", "fs_1", "tp_0", "tp_1"))
    return jax.shard_map(
        on_device,
        mesh=split,
        in_specs=(
            P(FS, TP),
            P(FS, None),
            P(),
            P(FS, TP),
            P(FS, TP),
            P(FS, TP),
            P(FS, TP),
            P(FS, TP),
            P(),
            P(FS, TP),
            P(FS, TP),
            P(FS, TP),
        ),
        out_specs=(
            P(FS, TP),
            P(FS, TP),
            P(None, TP),
            P(FS, TP),
            P(FS, TP),
            P(FS, TP),
            P(FS, TP),
            P(None, TP),
            P(FS, TP),
            P(FS, TP),
        ),
        check_vma=False,
    )
```

profile of v0, /device:TPU:4, one launch (start us, length us, event | category | flops | bytes accessed | tf_op | source)
XLA Modules:
  0.0 218.8 jit_solution(8862395068048219859)
XLA Ops:
  7.2 0.7 all-gather.3.cloned.1.call-update
  7.9 0.8 copy-done
  8.8 1.6 fusion.14
  10.4 2.0 convolution_bitcast_fusion.1
  12.5 75.5 %all-gather.3.cloned.1.call-done = bf16[2048,1024]{0,1:T(8,128)(2,1)} async-done(((bf16[2048,32]{0,1:T(8,128)(2,1)}), bf16[2048,1024]{0,1:T(8,128)(2,1)}) %all-gather.3.cloned.1.call-update) | async-done | bytes 4194320 | tf_op jit(solution)/shard_map/all_gather | solution.py:115
  88.0 3.5 %fusion.15 = f32[2048,128]{1,0:T(8,128)S(1)} fusion(bf16[2048,1024]{0,1:T(8,128)(2,1)} %all-gather.3.cloned.1.call-done, bf16[1024,128]{1,0:T(8,128)(2,1)S(1)} %copy-done.1), kind=kOutput, calls=%fused_computation.31 | convolution fusion | flops 536870912 | bytes 5505024 | tf_op jit(solution)/shard_map/dot_general | solution.py:116
  91.5 1.0 convolution_bitcast_fusion
  92.5 0.8 reshape.29
  93.2 7.3 %all-to-all-start = ((f32[16,1,1024]{2,1,0:T(1,128)}), f32[16,1,1024]{2,1,0:T(1,128)S(1)}, u32[]{:S(2)}, u32[]{:S(2)}) async-start(f32[16,1,1024]{2,1,0:T(1,128)} %reshape.29), calls=%async_computation | async-start | bytes 131072 | tf_op jit(solution)/shard_map/all_to_all | solution.py:23
  100.5 5.5 %all-to-all-done = f32[16,1,1024]{2,1,0:T(1,128)S(1)} async-done(((f32[16,1,1024]{2,1,0:T(1,128)}), f32[16,1,1024]{2,1,0:T(1,128)S(1)}, u32[]{:S(2)}, u32[]{:S(2)}) %all-to-all-start) | async-done | bytes 65568 | tf_op jit(solution)/shard_map/all_to_all | solution.py:23
  106.0 0.5 broadcast.38
  106.6 0.8 reduce
  107.5 0.6 multiply_reduce_fusion.1
  108.1 9.5 %all-reduce.2 = (f32[]{:T(128)}, f32[]{:T(128)}) all-reduce(f32[]{:T(128)} %get-tuple-element.31, f32[]{:T(128)} %get-tuple-element.30), channel_id=1, replica_groups=mesh['fs_0'=4,'fs_1'=4,'tp_0'=16,'tp_1'=2] {'fs_0'}, use_global_device_ids=true, to_apply=%region_7.0 | all-reduce | flops 2 | bytes 16 | tf_op jit(solution)/shard_map/psum | solution.py:29
  117.6 9.1 %all-reduce.1 = (f32[]{:T(128)}, f32[]{:T(128)}) all-reduce(f32[]{:T(128)} %get-tuple-element.36, f32[]{:T(128)} %get-tuple-element.37), channel_id=1, replica_groups=mesh['fs_0'=4,'fs_1'=4,'tp_0'=16,'tp_1'=2] {'fs_1'}, use_global_device_ids=true, to_apply=%region_8.0 | all-reduce | flops 2 | bytes 16 | tf_op jit(solution)/shard_map/psum | solution.py:29
  126.6 30.3 %all-reduce = (f32[]{:T(128)}, f32[]{:T(128)}) all-reduce(f32[]{:T(128)} %get-tuple-element.34, f32[]{:T(128)} %get-tuple-element.35), channel_id=1, replica_groups=mesh['fs_0'=4,'fs_1'=4,'tp_0'=16,'tp_1'=2] {'tp_0'}, use_global_device_ids=true, to_apply=%region_9.0 | all-reduce | flops 2 | bytes 16 | tf_op jit(solution)/shard_map/psum | solution.py:29
  156.9 3.1 %all-reduce.3 = (f32[]{:T(128)}, f32[]{:T(128)}) all-reduce(f32[]{:T(128)} %get-tuple-element.32, f32[]{:T(128)} %get-tuple-element.33), channel_id=1, replica_groups=mesh['fs_0'=4,'fs_1'=4,'tp_0'=16,'tp_1'=2] {'tp_1'}, use_global_device_ids=true, to_apply=%region_10.0 | all-reduce | flops 2 | bytes 16 | tf_op jit(solution)/shard_map/psum | solution.py:29
  161.4 0.6 add_divide_fusion.1
  162.1 22.1 %all_gather.13 = f32[128,128]{1,0:T(8,128)S(1)} all-gather(f32[8,128]{1,0:T(8,128)S(1)} %pad_maximum_fusion.2), channel_id=1, replica_groups=mesh['fs_0'=4,'fs_1'=4,'tp_0'=16,'tp_1'=2] {'fs_0','fs_1'}, dimensions={0}, use_global_device_ids=true | all-gather | bytes 69632 | tf_op jit(solution)/shard_map/all_gather | solution.py:35
  184.2 0.9 fusion.11
  185.2 1.5 fusion.10
  186.7 23.2 %all-gather = bf16[98304]{0:T(1024)(128)(2,1)S(1)} all-gather(bf16[6144]{0:T(1024)(128)(2,1)S(1)} %pad_maximum_fusion.1), channel_id=2, replica_groups=mesh['fs_0'=4,'fs_1'=4,'tp_0'=16,'tp_1'=2] {'fs_0','fs_1'}, dimensions={0}, use_global_device_ids=true | all-gather | bytes 208896 | tf_op jit(solution)/shard_map/all_gather | solution.py:50
  210.3 0.8 copy.31
  211.2 0.7 copy.30
  (30 shorter events, 1.0 us)
Async XLA Ops:
  7.2 1.6 copy-start
  7.2 80.8 %copy-start.1 = (bf16[1024,128]{1,0:T(8,128)(2,1)S(1)}, bf16[1024,128]{1,0:T(8,128)(2,1)}, u32[]{:S(2)}) copy-start(bf16[1024,128]{1,0:T(8,128)(2,1)} %param.20) | copy-start | bytes 786436
  7.2 80.8 %all-gather.3.cloned.1.call-start = ((), (), s32[]{:S(2)}) async-start(), calls=%async_computation.1 | async-start | bytes 4325376 | tf_op jit(solution)/shard_map/all_gather | solution.py:115
  10.4 81.1 %copy-start.2 = (bf16[2048,64]{0,1:T(8,128)(2,1)S(1)}, bf16[2048,64]{0,1:T(8,128)(2,1)}, u32[]{:S(2)}) copy-start(bf16[2048,64]{0,1:T(8,128)(2,1)} %param.19) | copy-start | bytes 786436
  12.4 149.0 %copy-start.5 = (f32[8,64]{1,0:T(8,128)S(1)}, f32[8,64]{1,0:T(8,128)}, u32[]{:S(2)}) copy-start(f32[8,64]{1,0:T(8,128)} %param.17) | copy-start | bytes 6148
  12.4 149.0 %copy-start.6 = (f32[8,64]{1,0:T(8,128)S(1)}, f32[8,64]{1,0:T(8,128)}, u32[]{:S(2)}) copy-start(f32[8,64]{1,0:T(8,128)} %param.16) | copy-start | bytes 6148
  12.4 149.0 %copy-start.7 = (f32[8,64]{1,0:T(8,128)S(1)}, f32[8,64]{1,0:T(8,128)}, u32[]{:S(2)}) copy-start(f32[8,64]{1,0:T(8,128)} %param.23) | copy-start | bytes 6148
  12.4 149.0 %copy-start.8 = (f32[8,64]{1,0:T(8,128)S(1)}, f32[8,64]{1,0:T(8,128)}, u32[]{:S(2)}) copy-start(f32[8,64]{1,0:T(8,128)} %param.22) | copy-start | bytes 6148
  12.4 171.8 %copy-start.3 = (f32[64,64]{1,0:T(8,128)S(1)}, f32[64,64]{1,0:T(8,128)}, u32[]{:S(2)}) copy-start(f32[64,64]{1,0:T(8,128)} %param.21) | copy-start | bytes 49156
  12.4 172.7 %copy-start.4 = (f32[32,64]{1,0:T(8,128)S(1)}, f32[32,64]{1,0:T(8,128)}, u32[]{:S(2)}) copy-start(f32[32,64]{1,0:T(8,128)} %param.15) | copy-start | bytes 24580
  93.2 12.8 %all-to-all-start = ((f32[16,1,1024]{2,1,0:T(1,128)}), f32[16,1,1024]{2,1,0:T(1,128)S(1)}, u32[]{:S(2)}, u32[]{:S(2)}) async-start(f32[16,1,1024]{2,1,0:T(1,128)} %reshape.29), calls=%async_computation | async-start | bytes 131072 | tf_op jit(solution)/shard_map/all_to_all | solution.py:23
Sparse Core Ops, SparseCore 0:
  10.1 77.7 all-gather.2
where the time goes:
time: 219 us
  blocking collectives  97.2 us (44%)
  waiting for transfers between devices  81.7 us (37%)
  between operations  15.6 us (7%)
  matrix products  10.4 us (5%)
  starting transfers between devices  7.3 us (3%)
  local copies, waits for them, and re-layouts  4.46 us (2%)
    all_gather x1, waiting for transfers between devices, on_device(): heads_whole = lax.all_gather(mixed_heads, TP, axis=1, tiled=True)  75.5 us
    psum x4, blocking collectives, by_axis(): x = lax.psum(x, axis)  51.9 us
    all_gather x1, blocking collectives, gather_packed(): lines, at, outs = (lax.all_gather(flat, axis), 0, [])  23.2 us
    all_gather x1, blocking collectives, in_one_piece(): whole, at, outs = (lax.all_gather(both, axis, axis=dim, tiled=True), 0, [])  22.1 us
    all_to_all x1, starting transfers between devices, summed_on_arrival(): tiles = lax.all_to_all(split_up(x, dim, count), axis, 0, 0, tiled=True)  7.27 us
    all_to_all x1, waiting for transfers between devices, summed_on_arrival(): tiles = lax.all_to_all(split_up(x, dim, count), axis, 0, 0, tiled=True)  5.54 us
  transfers between devices with their start and end apart: 2, of which 2 were waited for; matrix products, arithmetic and copies ran while one was open for 2% of the time, Pallas kernels for 0%

commit v1 on v0

v1 whole, which is shorter than its diff:
```python
import functools

import jax
import jax.numpy as jnp
from jax import lax
from jax.experimental import pallas as pl
from jax.experimental.pallas import tpu as pltpu
from jax.sharding import PartitionSpec as P

MESH = pl.DeviceIdType.MESH
f32 = jnp.float32
bf16 = jnp.bfloat16
NT = (((1,), (1,)), ((), ()))


def two_parts(x):
    hi = x.astype(bf16)
    return hi, (x - hi.astype(f32)).astype(bf16)


def dot(a, b):
    return jnp.dot(a, b, preferred_element_type=f32)


def dot_nt(a, b):
    return lax.dot_general(a, b, NT, preferred_element_type=f32)


def exact_dot(x, w):
    hi, lo = two_parts(x)
    return dot(hi, w) + dot(lo, w)


def rcopy(src, dst, send, recv, device):
    return pltpu.make_async_remote_copy(
        src_ref=src,
        dst_ref=dst,
        send_sem=send,
        recv_sem=recv,
        device_id=device,
        device_id_type=MESH,
    )


def main_kernel(
    nf,
    nz,
    total_count,
    vi_h,
    vc_h,
    fv_h,
    vm_h,
    vf_h,
    vs_h,
    mh_h,
    oc_h,
    fo_h,
    om_h,
    of_h,
    os_h,
    vstep_o,
    vnew_o,
    vcopy_o,
    vfirst_o,
    vsecond_o,
    ostep_o,
    onew_o,
    ocopy_o,
    ofirst_o,
    osecond_o,
    heads,
    vi,
    vc,
    fv,
    vm,
    vf,
    vs,
    oc,
    fo,
    om,
    of,
    os_,
    packs,
    acc,
    part_v,
    part_o,
    rs_v,
    rs_o,
    ag_v,
    ag_o,
    zrow,
    mt_v,
    mt_o,
    mom,
    pt_full,
    load_sem,
    ring_send,
    ring_recv,
    pn_send,
    pn_recv,
    fs_send,
    fs_recv,
    z_send,
    z_recv,
):
    me_f = lax.axis_index("fs")
    me_t = lax.axis_index("tp")
    z = me_t // 2
    core = lax.rem(me_t, 2)
    other = 1 - core
    half = nz // 2
    right = (me_f, lax.rem(z + 1, nz) * 2 + core)
    left = (me_f, lax.rem(z + nz - 1, nz) * 2 + core)
    partner = (me_f, z * 2 + other)

    def fs_dev(k):
        return lax.rem(me_f + k, nf)

    pairs = [
        (mh_h.at[0], heads.at[z, core, 0]),
        (mh_h.at[1], heads.at[z, core, 1]),
        (vf_h, vf),
        (vs_h, vs),
        (of_h, of),
        (os_h, os_),
        (vm_h, vm),
        (om_h, om),
        (vi_h, vi),
        (vc_h, vc),
        (fv_h, fv),
        (oc_h, oc),
        (fo_h, fo),
    ]
    loads = [pltpu.make_async_copy(s, d, load_sem.at[n]) for n, (s, d) in enumerate(pairs)]
    for cp in loads:
        cp.start()

    barrier = pltpu.get_barrier_semaphore()
    for dev in (left, right, partner):
        pl.semaphore_signal(barrier, inc=1, device_id=dev, device_id_type=MESH)
    for k in range(1, nf):
        pl.semaphore_signal(barrier, inc=1, device_id=(fs_dev(k), me_t), device_id_type=MESH)
    pl.semaphore_wait(barrier, 3 + nf - 1)

    def chip_at(d, s):
        return lax.rem(z + (nz - s if d == 0 else s), nz)

    def has(s, c, d):
        return s < half or c == d

    def ring_out(d, s, c):
        ref = heads.at[chip_at(d, s - 1), core, c]
        dev = right if d == 0 else left
        return rcopy(ref, ref, ring_send.at[d, s - 1, c], ring_recv.at[d, s - 1, c], dev)

    def ring_in(d, s, c):
        ref = heads.at[chip_at(d, s), core, c]
        dev = right if d == 0 else left
        return rcopy(ref, ref, ring_send.at[d, s - 1, c], ring_recv.at[d, s - 1, c], dev)

    def pn_out(d, s, c):
        ref = heads.at[chip_at(d, s), core, c]
        return rcopy(ref, ref, pn_send.at[d, s, c], pn_recv.at[d, s, c], partner)

    def pn_in(d, s, c):
        ref = heads.at[chip_at(d, s), other, c]
        return rcopy(ref, ref, pn_send.at[d, s, c], pn_recv.at[d, s, c], partner)

    sent = []

    def send(cp):
        cp.start()
        sent.append(cp)

    for c in range(2):
        loads[c].wait()
        for d in range(2):
            send(ring_out(d, 1, c))
    for c in range(2):
        send(pn_out(0, 0, c))

    for n in range(2, 8):
        loads[n].wait()
    own_v = jnp.concatenate([vf[...], vs[...], of[...], os_[...], vm[...]], axis=0)
    packs[me_f] = jnp.concatenate([own_v, om[...]], axis=1)

    def exchange(n, src, dst):
        for k in range(1, nf):
            send(rcopy(src(k), dst.at[me_f], fs_send.at[n, k], fs_recv.at[n, k], (fs_dev(k), me_t)))

    def arrive(n, dst):
        for k in range(1, nf):
            ref = dst.at[lax.rem(me_f + nf - k, nf)]
            rcopy(ref, ref, fs_send.at[n, k], fs_recv.at[n, k], (fs_dev(k), me_t)).wait_recv()

    exchange(0, lambda k: packs.at[me_f], packs)

    def scatter(n, part, rs, value):
        for i in range(nf):
            part[i] = value[4 * i : 4 * i + 4]
        rs[me_f] = part[me_f]
        exchange(n, lambda k: part.at[fs_dev(k)], rs)

    def gather(n, rs, ag):
        band = rs[0]
        for i in range(1, nf):
            band = band + rs[i]
        ag[me_f] = band
        exchange(n, lambda k: ag.at[me_f], ag)

    for n in range(8, 11):
        loads[n].wait()
    gv = dot(vi[...], vc[...])
    scatter(1, part_v, rs_v, exact_dot(gv, fv[...]))
    for n in range(11, 13):
        loads[n].wait()
    acc[...] = jnp.zeros_like(acc)

    def contribute(d, s):
        chip = chip_at(d, s)
        block = heads[chip].reshape(64, heads.shape[-1])
        g = dot_nt(oc[...], block)
        acc[...] += exact_dot(g, fo[pl.ds(pl.multiple_of(chip * 64, 64), 64), :])

    def partner_arrived(s):
        for c in range(2):
            for d in range(2):
                if (s > 0 or d == 0) and has(s, c, d):
                    pn_in(d, s, c).wait_recv()

    for s in range(1, half + 1):
        for c in range(2):
            for d in range(2):
                if has(s, c, d):
                    ring_in(d, s, c).wait_recv()
                    if s < half and has(s + 1, c, d):
                        send(ring_out(d, s + 1, c))
                    send(pn_out(d, s, c))
        partner_arrived(s - 1)
        contribute(0, s - 1)
        if s > 1:
            contribute(1, s - 1)
        if s == 2:
            arrive(1, rs_v)
            gather(2, rs_v, ag_v)
        if s == 3:
            arrive(0, packs)
            mt_v[...] = packs[:, 32:64, 0:64].reshape(nf * 32, 64).T
        if s == 4:
            mt_o[...] = packs[:, :, 64:128].reshape(nf * 64, 64).T
        if s == 5:
            for n in range(4):
                mom[n] = packs[:, 8 * n : 8 * n + 8, 0:64].reshape(nf * 8, 64).T
        if s == 6:
            arrive(2, ag_v)
    partner_arrived(half)
    contribute(0, half)

    scatter(3, part_o, rs_o, acc[...])
    arrive(3, rs_o)
    gather(4, rs_o, ag_o)
    arrive(4, ag_o)

    def whole(ag):
        return jnp.concatenate([ag[i] for i in range(nf)], axis=0)

    pv = whole(ag_v)
    po = whole(ag_o)

    def folded(p):
        row = jnp.sum(p * p, axis=0, keepdims=True)
        return row[:, :64] + row[:, 64:]

    zrow[me_t] = jnp.concatenate([folded(pv), folded(po)], axis=1)
    order = sorted(range(1, 2 * nz), key=lambda k: -min(k, 2 * nz - k))
    for k in order:
        dev = (me_f, lax.rem(me_t + k, 2 * nz))
        send(rcopy(zrow.at[me_t], zrow.at[me_t], z_send.at[k], z_recv.at[k], dev))
    pt_full[0] = pv.T
    pt_full[1] = po.T
    at8 = pl.ds(pl.multiple_of(me_f * 8, 8), 8)
    band_v = pt_full[0, at8, :]
    band_o = pt_full[1, at8, :]
    for k in order:
        ref = zrow.at[lax.rem(me_t + 2 * nz - k, 2 * nz)]
        dev = (me_f, lax.rem(me_t + k, 2 * nz))
        rcopy(ref, ref, z_send.at[k], z_recv.at[k], dev).wait_recv()
    rows = zrow[0]
    for j in range(1, 2 * nz):
        rows = rows + zrow[j]
    scale_v = lax.rsqrt(jnp.sum(rows[:, :64], axis=1, keepdims=True) / total_count + 1e-06)
    scale_o = lax.rsqrt(jnp.sum(rows[:, 64:], axis=1, keepdims=True) / total_count + 1e-06)

    def update(projected, scale, first, second):
        scaled = scale * projected
        first_new = 0.9 * first + 0.1 * scaled
        second_new = 0.95 * second + 0.05 * scaled * scaled
        return first_new, second_new

    def finish(p, band, scale, n, first, second, factor, mt, master, step_o, new_o, copy_o, first_o, second_o):
        first_new, second_new = update(p, scale, mom[n], mom[n + 1])
        direction = first_new / (jnp.sqrt(second_new) + 1e-08)
        hi, lo = two_parts(direction)
        w = factor[...]
        step_t = dot_nt(hi, w) + dot_nt(lo, w)
        copy_o[...] = (mt[...] - 0.002 * step_t).astype(bf16)
        count = master.shape[0]
        block = factor[pl.ds(pl.multiple_of(me_f * count, count), count), :]
        step = dot_nt(block, hi) + dot_nt(block, lo)
        step_o[...] = step
        new_o[...] = master[...] - 0.002 * step
        first_o[...], second_o[...] = update(band, scale, first[...], second[...])

    finish(pv, band_v, scale_v, 0, vf, vs, fv, mt_v, vm, vstep_o, vnew_o, vcopy_o, vfirst_o, vsecond_o)
    finish(po, band_o, scale_o, 2, of, os_, fo, mt_o, om, ostep_o, onew_o, ocopy_o, ofirst_o, osecond_o)

    for cp in sent:
        cp.wait_send()


def export_kernel(*refs):
    count = (len(refs) - 1) // 2
    ins, outs, sem = refs[:count], refs[count : 2 * count], refs[-1]
    copies = [pltpu.make_async_copy(a, b, sem.at[n]) for n, (a, b) in enumerate(zip(ins, outs))]
    for cp in copies:
        cp.start()
    for cp in copies:
        cp.wait()


def on_device(nf, nz, vi, vc, fv, vm, vf, vs, mh, oc, fo, om, of, os_):
    tokens, columns = vi.shape
    rank = fv.shape[1]
    total_count = rank * columns * nz * 2
    f_rows, o_rows = fv.shape[0], fo.shape[0]

    def out(shape, dtype):
        return jax.ShapeDtypeStruct(shape, dtype)

    outs = (
        out(vm.shape, f32),
        out(vm.shape, f32),
        out((columns, f_rows), bf16),
        out(vf.shape, f32),
        out(vf.shape, f32),
        out(om.shape, f32),
        out(om.shape, f32),
        out((columns, o_rows), bf16),
        out(of.shape, f32),
        out(of.shape, f32),
    )
    V = pltpu.VMEM
    D = pltpu.SemaphoreType.DMA
    half = nz // 2
    scratch = [
        V((nz, 2, 2, 16, tokens), bf16),
        V((columns, tokens), bf16),
        V(vc.shape, bf16),
        V(fv.shape, bf16),
        V(vm.shape, f32),
        V(vf.shape, f32),
        V(vs.shape, f32),
        V((columns, tokens), bf16),
        V(fo.shape, bf16),
        V(om.shape, f32),
        V(of.shape, f32),
        V(os_.shape, f32),
        V((nf, 64, 128), f32),
        V((columns, rank), f32),
        V((nf, 4, 128), f32),
        V((nf, 4, 128), f32),
        V((nf, 4, 128), f32),
        V((nf, 4, 128), f32),
        V((nf, 4, 128), f32),
        V((nf, 4, 128), f32),
        V((2 * nz, 1, 128), f32),
        V((columns, f_rows), f32),
        V((columns, o_rows), f32),
        V((4, columns, rank), f32),
        V((2, rank, columns), f32),
        D((13,)),
        D((2, half, 2)),
        D((2, half, 2)),
        D((2, half + 1, 2)),
        D((2, half + 1, 2)),
        D((5, nf)),
        D((5, nf)),
        D((2 * nz,)),
        D((2 * nz,)),
    ]
    hbm = pl.BlockSpec(memory_space=pltpu.MemorySpace.HBM)
    vmem = pl.BlockSpec(memory_space=pltpu.VMEM)
    results = pl.pallas_call(
        functools.partial(main_kernel, nf, nz, total_count),
        out_shape=outs,
        in_specs=[hbm] * 12,
        out_specs=(vmem,) * 10,
        scratch_shapes=scratch,
        compiler_params=pltpu.CompilerParams(
            collective_id=0, has_side_effects=True, vmem_limit_bytes=32 * 1024 * 1024
        ),
        name="main",
    )(vi.T, vc, fv, vm, vf, vs, mh.T.reshape(2, 16, tokens), oc.T, fo, om, of, os_)
    results = pl.pallas_call(
        export_kernel,
        out_shape=outs,
        in_specs=[vmem] * 10,
        out_specs=(hbm,) * 10,
        scratch_shapes=[D((10,))],
        compiler_params=pltpu.CompilerParams(vmem_limit_bytes=16 * 1024 * 1024),
        name="export",
    )(*results)
    results = list(results)
    results[2] = results[2].T
    results[7] = results[7].T
    return tuple(results)


def solution(mesh):
    both = P("fs", "tp")
    cols = P(None, "tp")
    return jax.shard_map(
        functools.partial(on_device, mesh.shape["fs"], mesh.shape["tp"] // 2),
        mesh=mesh,
        in_specs=(both, P("fs", None), P(), both, both, both, both, both, P(), both, both, both),
        out_specs=(both, both, cols, both, both, both, both, cols, both, both),
        check_vma=False,
    )
```

time: 219 us -> 81.2 us (0.37)
  the two profiles are of different devices: /device:TPU:4 before, /device:TPU:1 now
where the time goes in v1:
time: 81.2 us; the launch traced here: 80.7 us
  Pallas kernels  69.5 us (86%)
  local copies, waits for them, and re-layouts  10.5 us (13%)
    pallas_call x1, Pallas kernels, on_device(): pl.pallas_call(functools.partial(main_kernel, nf, nz, total_count), out_s...  68.7 us
    unnamed x24, local copies, waits for them, and re-layouts  10.5 us

profile of v1, /device:TPU:1, one launch (start us, length us, event | category | flops | bytes accessed | tf_op | source)
XLA Modules:
  0.0 80.7 jit_solution(4388505380962659442)
XLA Ops:
  0.6 0.0 copy-start
  0.7 1.6 %copy-done = bf16[2048,512]{1,0:T(8,128)(2,1)S(1)} copy-done((bf16[2048,512]{1,0:T(8,128)(2,1)S(1)}, bf16[2048,512]{1,0:T(8,128)(2,1)}, u32[]{:S(2)}) %copy-start) | copy-done | bytes 2097176
  2.2 0.0 copy-start.1
  2.2 0.9 %copy-done.1 = bf16[2048,64]{0,1:T(8,128)(2,1)S(1)} copy-done((bf16[2048,64]{0,1:T(8,128)(2,1)S(1)}, bf16[2048,64]{0,1:T(8,128)(2,1)}, u32[]{:S(2)}) %copy-start.1) | copy-done | bytes 262168
  3.2 0.0 copy-start.2
  3.2 0.9 %copy-done.2 = bf16[2048,64]{0,1:T(8,128)(2,1)S(1)} copy-done((bf16[2048,64]{0,1:T(8,128)(2,1)S(1)}, bf16[2048,64]{0,1:T(8,128)(2,1)}, u32[]{:S(2)}) %copy-start.2) | copy-done | bytes 262168
  4.1 0.0 copy-start.3
  4.1 0.9 %copy-done.3 = bf16[1024,128]{1,0:T(8,128)(2,1)S(1)} copy-done((bf16[1024,128]{1,0:T(8,128)(2,1)S(1)}, bf16[1024,128]{1,0:T(8,128)(2,1)}, u32[]{:S(2)}) %copy-start.3) | copy-done | bytes 262168
  5.1 0.0 copy-start.4
  5.1 0.9 %copy-done.4 = bf16[512,128]{1,0:T(8,128)(2,1)S(1)} copy-done((bf16[512,128]{1,0:T(8,128)(2,1)S(1)}, bf16[512,128]{1,0:T(8,128)(2,1)}, u32[]{:S(2)}) %copy-start.4) | copy-done | bytes 131096
  6.0 0.0 copy-start.5
  6.0 0.9 %copy-done.5 = bf16[2048,32]{0,1:T(8,128)(2,1)S(1)} copy-done((bf16[2048,32]{0,1:T(8,128)(2,1)S(1)}, bf16[2048,32]{0,1:T(8,128)(2,1)}, u32[]{:S(2)}) %copy-start.5) | copy-done | bytes 131096
  6.9 0.0 copy-start.6
  6.9 0.8 copy-done.6
  7.7 0.0 copy-start.7
  7.7 0.7 copy-done.7
  8.4 0.0 copy-start.8
  8.4 0.7 copy-done.8
  9.1 0.0 copy-start.9
  9.1 0.7 copy-done.9
  9.8 0.7 copy-done.10
  10.4 0.7 copy-done.11
  11.1 68.7 %main.1 = (f32[32,64]{1,0:T(8,128)S(1)}, f32[32,64]{1,0:T(8,128)S(1)}, bf16[64,512]{1,0:T(8,128)(2,1)S(1)}, f32[8,64]{1,0:T(8,128)S(1)}, f32[8,64]{1,0:T(8,128)S...) custom-call(bf16[64,2048]{1,0:T(8,128)(2,1)S(1)} %bitcast.7, ...), custom_call_target="tpu_custom_call" | custom-call | tf_op jit(solution)/shard_map/main/pallas_call | solution.py:393
  79.9 0.8 %export.1 = (f32[32,64]{1,0:T(8,128)}, f32[32,64]{1,0:T(8,128)}, bf16[64,512]{1,0:T(8,128)(2,1)}, f32[8,64]{1,0:T(8,128)}, f32[8,64]{1,0:T(8,128)}, /*index=5*/f...) custom-call(f32[32,64]{1,0:T(8,128)S(1)} %get-tuple-element.30.refs_0_, ...), custom_call_target="tpu_custom_call" | custom-call | tf_op jit(solution)/shard_map/export/pallas_call | solution.py:404
  (2 shorter events, 0.0 us)
Async XLA Ops:
  0.6 1.6 %copy-start = (bf16[2048,512]{1,0:T(8,128)(2,1)S(1)}, bf16[2048,512]{1,0:T(8,128)(2,1)}, u32[]{:S(2)}) copy-start(bf16[2048,512]{1,0:T(8,128)(2,1)} %vc_h.1) | copy-start | bytes 6291460
  2.2 0.9 %copy-start.1 = (bf16[2048,64]{0,1:T(8,128)(2,1)S(1)}, bf16[2048,64]{0,1:T(8,128)(2,1)}, u32[]{:S(2)}) copy-start(bf16[2048,64]{0,1:T(8,128)(2,1)} %param.12) | copy-start | bytes 786436
  3.2 0.9 %copy-start.2 = (bf16[2048,64]{0,1:T(8,128)(2,1)S(1)}, bf16[2048,64]{0,1:T(8,128)(2,1)}, u32[]{:S(2)}) copy-start(bf16[2048,64]{0,1:T(8,128)(2,1)} %param.19) | copy-start | bytes 786436
  4.1 0.9 %copy-start.3 = (bf16[1024,128]{1,0:T(8,128)(2,1)S(1)}, bf16[1024,128]{1,0:T(8,128)(2,1)}, u32[]{:S(2)}) copy-start(bf16[1024,128]{1,0:T(8,128)(2,1)} %fo_h.1) | copy-start | bytes 786436
  5.1 0.9 %copy-start.4 = (bf16[512,128]{1,0:T(8,128)(2,1)S(1)}, bf16[512,128]{1,0:T(8,128)(2,1)}, u32[]{:S(2)}) copy-start(bf16[512,128]{1,0:T(8,128)(2,1)} %fv_h.1) | copy-start | bytes 393220
  6.0 0.9 %copy-start.5 = (bf16[2048,32]{0,1:T(8,128)(2,1)S(1)}, bf16[2048,32]{0,1:T(8,128)(2,1)}, u32[]{:S(2)}) copy-start(bf16[2048,32]{0,1:T(8,128)(2,1)} %param.18) | copy-start | bytes 393220
  6.9 0.8 copy-start.6
  7.7 0.7 copy-start.7
  8.4 0.7 copy-start.8
  9.1 0.7 copy-start.9
  9.8 0.7 copy-start.10
  10.4 0.7 copy-start.11
